TPU v7x, 768 devices: a whole 4x8x12 slice. The times are simulated.
768 devices in a mesh: rep: 3 (over z_hi), fs: 32 (over z_lo, y), tp: 8 (over x, core).
Axes of the slice: x: 4, y: 8, z: 12 (z_hi: 3, z_lo: 4; z = z_hi * 4 + z_lo), core: 2. Of those that a mesh axis runs over, the one named last changes fastest.
Arguments:
- gate_pre: bfloat16 [98304, 3072], P(('rep', 'fs'), 'tp'), may hold values from -6 to 6
- up_pre: bfloat16 [98304, 3072], P(('rep', 'fs'), 'tp'), may hold values from -6 to 6
- out_grad: bfloat16 [98304, 2048], P(('rep', 'fs')), may hold values from -8 to 8
- w_down: bfloat16 [3072, 2048], P('tp', 'fs'), may hold values from -0.109375 to 0.109375
Outputs:
- d_gate: bfloat16 [98304, 3072], P(('rep', 'fs'), 'tp')
- d_up: bfloat16 [98304, 3072], P(('rep', 'fs'), 'tp')
- grad_down: float32 [3072, 2048], P('tp', 'fs')
- row_energy: float32 [3072], P('tp')
All inputs are finite; a program needn't handle non-finite values.
Results may differ from a plain program's by a relative error of at most 0.0034.
Values may be sent and summed in bfloat16 or wider, within the bound.
No kernel may reach another device: no remote copies, remote signals or barrier semaphores. Data moves between devices by JAX's collectives and lax.ppermute only.
A program may use at most 32 MiB of HBM per device.

v0:
```python
import jax
import jax.numpy as jnp
from jax import lax
from jax.sharding import Mesh
from jax.sharding import PartitionSpec as P

D = 2048
FS = ("fs_0", "fs_1")
REP_FS = ("rep", "fs_0", "fs_1")


def from_everyone(value, axis):
    peers = lax.axis_size(axis)
    return lax.all_to_all(
        jnp.broadcast_to(value[None], (peers, *value.shape)), axis, 0, 0, tiled=True
    )


def joined_along(blocks, dim):
    dims = list(blocks.shape[1:])
    dims[dim] *= blocks.shape[0]
    return jnp.moveaxis(blocks, 0, dim).reshape(dims)


def collect(value, axis, dim):
    blocks = from_everyone(value, axis)
    return joined_along(blocks, dim)


def sum_in_order(blocks, axes, order):
    dims = [lax.axis_size(a) for a in axes]
    blocks = blocks.reshape(*dims, *blocks.shape[1:])
    blocks = blocks.transpose(*order, *range(len(axes), blocks.ndim))
    blocks = blocks.reshape(-1, *blocks.shape[len(axes) :])
    for k in order:
        blocks = lax.psum_scatter(blocks, axes[k], scatter_dimension=0, tiled=True)
    return blocks[0]


def split_up(value, dim, peers):
    before, after = (value.shape[:dim], value.shape[dim + 1 :])
    return jnp.moveaxis(value.reshape(*before, peers, -1, *after), dim, 0)


def sum_by_axis(value, axes, order, dim):
    peers = lax.axis_size(axes)
    return sum_in_order(split_up(value, dim, peers), axes, order)


def over_copies(value, axis):
    return from_everyone(value, axis).sum(axis=0)


def local(gate_pre, up_pre, out_grad, w_down):
    gate_f = gate_pre.astype(jnp.float32)
    up_f = up_pre.astype(jnp.float32)
    sig = jax.nn.sigmoid(gate_f)
    act = gate_f * sig
    hidden = (act * up_f).astype(jnp.bfloat16)
    tokens_all = out_grad.shape[0] * lax.axis_size("rep") * lax.axis_size(FS)
    factor = float(tokens_all) ** (-0.5)
    weight_whole = collect(w_down, FS, 1)
    dhid = lax.dot_general(
        out_grad, weight_whole, (((1,), (1,)), ((), ())), preferred_element_type=jnp.float32
    )
    d_up = (dhid * act).astype(jnp.bfloat16)
    d_gate = (dhid * up_f * sig * (1.0 + gate_f * (1.0 - sig))).astype(jnp.bfloat16)
    d_gate, d_up = (d_gate, d_up)
    shard = sum_by_axis(
        lax.dot_general(
            out_grad, hidden, (((0,), (0,)), ((), ())), preferred_element_type=jnp.float32
        ),
        FS,
        (1, 0),
        0,
    )
    shard = over_copies(shard, "rep")
    grad_down = shard.T * factor
    energy = over_copies(jnp.sum(grad_down * grad_down, axis=1), FS) / D
    return (d_gate, d_up, grad_down, energy)


def solution(mesh):
    torus = Mesh(
        mesh.devices.reshape(mesh.shape["rep"], 4, 8, mesh.shape["tp"]),
        ("rep", "fs_0", "fs_1", "tp"),
    )
    placed = (P(REP_FS, "tp"), P(REP_FS, "tp"), P(REP_FS, None), P("tp", FS))
    return jax.shard_map(
        local,
        mesh=torus,
        in_specs=placed,
        out_specs=(P(REP_FS, "tp"), P(REP_FS, "tp"), P("tp", FS), P("tp")),
        check_vma=False,
    )
```

profile of v0, /device:TPU:4, one launch (start us, length us, event | category | flops | bytes accessed | tf_op | source)
XLA Modules:
  0.0 206.1 jit_solution(17777173379978953035)
XLA Ops:
  7.2 0.0 reduce-scatter.3.cloned.1.call-start
  7.2 6.3 %convolution_bitcast_fusion = f32[2048,384]{0,1:T(8,128)} fusion(bf16[1024,2048]{1,0:T(8,128)(2,1)} %param.6, bf16[1024,384]{1,0:T(8,128)(2,1)} %param.5, bf16[1024,384]{1,0:T(8,128)(2,1)} %param.4), kind=kOutput, calls=%fused_computation | convolution fusion | flops 1613758464 | bytes 8912896 | tf_op jit(solution)/shard_map/dot_general | solution.py:70
  13.5 2.4 %copy.13 = f32[2048,384]{1,0:T(8,128)S(1)} copy(f32[2048,384]{0,1:T(8,128)} %convolution_bitcast_fusion) | data formatting | bytes 6291456 | tf_op jit(solution)/shard_map/dot_general | solution.py:70
  15.9 1.9 copy.14
  17.7 0.0 copy-start
  17.7 0.0 reduce-scatter.3.cloned.1.call-update
  17.8 0.0 reduce-scatter.5.cloned.1.call-start
  17.8 58.9 %reduce-scatter.3.cloned.1.call-done = f32[4,64,384]{2,1,0:T(8,128)} async-done(((f32[32,64,384]{2,1,0:T(8,128)}), f32[4,64,384]{2,1,0:T(8,128)}) %reduce-scatter.3.cloned.1.call-update) | async-done | bytes 393232 | tf_op jit(solution)/shard_map/reduce_scatter | solution.py:36
  76.7 0.0 reduce-scatter.5.cloned.1.call-update
  76.7 35.0 %reduce-scatter.5.cloned.1.call-done = f32[1,64,384]{2,1,0:T(8,128)} async-done(((f32[4,64,384]{2,1,0:T(8,128)}), f32[1,64,384]{2,1,0:T(8,128)}) %reduce-scatter.5.cloned.1.call-update) | async-done | bytes 98320 | tf_op jit(solution)/shard_map/reduce_scatter | solution.py:36
  111.7 0.9 broadcast_in_dim.10
  112.7 19.8 %all_to_all.16 = f32[3,64,384]{2,1,0:T(8,128)S(1)} all-to-all(f32[3,64,384]{2,1,0:T(8,128)S(1)} %broadcast_in_dim.10), channel_id=1, replica_groups=mesh['rep'=3,'fs_0'=4,'fs_1'=8,'tp'=8] {'rep'}, dimensions={0} | all-to-all | bytes 589824 | tf_op jit(solution)/shard_map/all_to_all | solution.py:14
  132.5 0.0 copy-done
  132.5 1.4 broadcast_in_dim.8
  133.8 0.0 copy-start.1
  133.9 0.0 copy-start.2
  133.9 7.8 %all-to-all-start = ((bf16[32,384,64]{1,2,0:T(8,128)(2,1)}), bf16[32,384,64]{1,2,0:T(8,128)(2,1)S(1)}, u32[]{:S(2)}, u32[]{:S(2)}) async-start(bf16[32,384,64]{1,2,0:T(8,128)(2,1)} %broadcast_in_dim.8), calls=%async_computation | async-start | bytes 3145728 | tf_op jit(solution)/shard_map/all_to_all | solution.py:14
  141.7 0.7 multiply_reduce_fusion
  142.4 39.1 %all-to-all-done = bf16[32,384,64]{1,2,0:T(8,128)(2,1)S(1)} async-done(((bf16[32,384,64]{1,2,0:T(8,128)(2,1)}), bf16[32,384,64]{1,2,0:T(8,128)(2,1)S(1)}, u32[]{:S(2)}, u32[]{:S(2)}) %all-to-all-start) | async-done | bytes 1572896 | tf_op jit(solution)/shard_map/all_to_all | solution.py:14
  181.5 0.6 broadcast_in_dim.22
  182.1 6.3 %all-to-all-start.2 = ((f32[32,1,384]{2,1,0:T(1,128)}), f32[32,1,384]{2,1,0:T(1,128)S(1)}, u32[]{:S(2)}, u32[]{:S(2)}) async-start(f32[32,1,384]{2,1,0:T(1,128)} %broadcast_in_dim.22), calls=%async_computation.4 | async-start | bytes 98304 | tf_op jit(solution)/shard_map/all_to_all | solution.py:14
  188.4 0.0 copy-done.1
  188.4 0.0 copy-done.2
  188.4 6.1 %multiply_convert_fusion = (bf16[1024,384]{1,0:T(8,128)(2,1)}, bf16[1024,384]{1,0:T(8,128)(2,1)}) fusion(bf16[1024,384]{1,0:T(8,128)(2,1)S(1)} %copy-done.1, bf16[1024,384]{1,0:T(8,128)(2,1)S(1)} %copy-done.2, bf16[1024,2048]{1,0:T(8,128)(2,1)} %param.6, bf16[384,2048]{0,1:T(8,128)(2,1)S(1)} %bitcast.18), kind=kOutput, calls=%fused_computation.14 | convolution fusion | flops 1616510976 | bytes 8912896 | tf_op jit(solution)/shard_map/dot_general | solution.py:63
  194.5 4.1 %all-to-all-done.2 = f32[32,1,384]{2,1,0:T(1,128)S(1)} async-done(((f32[32,1,384]{2,1,0:T(1,128)}), f32[32,1,384]{2,1,0:T(1,128)S(1)}, u32[]{:S(2)}, u32[]{:S(2)}) %all-to-all-start.2) | async-done | bytes 49184 | tf_op jit(solution)/shard_map/all_to_all | solution.py:14
  198.6 0.1 reduce_sum.29
  198.7 0.6 broadcast_multiply_fusion
  (1 shorter events, 0.0 us)
Async XLA Ops:
  7.2 69.6 %reduce-scatter.3.cloned.1.call-start = ((), (), s32[]{:S(2)}) async-start(), calls=%async_computation.5 | async-start | bytes 3538944 | tf_op jit(solution)/shard_map/reduce_scatter | solution.py:36
  17.7 114.7 %copy-start = (bf16[384,64]{0,1:T(8,128)(2,1)S(1)}, bf16[384,64]{0,1:T(8,128)(2,1)}, u32[]{:S(2)}) copy-start(bf16[384,64]{0,1:T(8,128)(2,1)} %param.7) | copy-start | bytes 147460
  17.8 94.0 %reduce-scatter.5.cloned.1.call-start = ((), (), s32[]{:S(2)}) async-start(), calls=%async_computation.6 | async-start | bytes 491520 | tf_op jit(solution)/shard_map/reduce_scatter | solution.py:36
  133.8 54.5 %copy-start.1 = (bf16[1024,384]{1,0:T(8,128)(2,1)S(1)}, bf16[1024,384]{1,0:T(8,128)(2,1)}, u32[]{:S(2)}) copy-start(bf16[1024,384]{1,0:T(8,128)(2,1)} %param.4) | copy-start | bytes 2359300
  133.9 54.5 %copy-start.2 = (bf16[1024,384]{1,0:T(8,128)(2,1)S(1)}, bf16[1024,384]{1,0:T(8,128)(2,1)}, u32[]{:S(2)}) copy-start(bf16[1024,384]{1,0:T(8,128)(2,1)} %param.5) | copy-start | bytes 2359300
  133.9 47.6 %all-to-all-start = ((bf16[32,384,64]{1,2,0:T(8,128)(2,1)}), bf16[32,384,64]{1,2,0:T(8,128)(2,1)S(1)}, u32[]{:S(2)}, u32[]{:S(2)}) async-start(bf16[32,384,64]{1,2,0:T(8,128)(2,1)} %broadcast_in_dim.8), calls=%async_computation | async-start | bytes 3145728 | tf_op jit(solution)/shard_map/all_to_all | solution.py:14
  182.1 16.5 %all-to-all-start.2 = ((f32[32,1,384]{2,1,0:T(1,128)}), f32[32,1,384]{2,1,0:T(1,128)S(1)}, u32[]{:S(2)}, u32[]{:S(2)}) async-start(f32[32,1,384]{2,1,0:T(1,128)} %broadcast_in_dim.22), calls=%async_computation.4 | async-start | bytes 98304 | tf_op jit(solution)/shard_map/all_to_all | solution.py:14
Sparse Core Ops, SparseCore 0:
  17.9 58.7 reduce-scatter.2
  79.8 31.8 reduce-scatter.4
where the time goes:
time: 206 us
  waiting for transfers between devices  137 us (67%)
  blocking collectives  19.8 us (10%)
  starting transfers between devices  14.2 us (7%)
  between operations  14.1 us (7%)
  matrix products  12.4 us (6%)
  local copies, waits for them, and re-layouts  7.22 us (4%)
    reduce_scatter x2, waiting for transfers between devices, sum_in_order(): blocks = lax.psum_scatter(blocks, axes[k], scatter_dimension=0, tiled=True)  93.9 us
    all_to_all x2, waiting for transfers between devices, from_everyone(): lax.all_to_all(jnp.broadcast_to(value[None], (peers, *value.shape)), axis...  43.2 us
    all_to_all x1, blocking collectives, from_everyone(): lax.all_to_all(jnp.broadcast_to(value[None], (peers, *value.shape)), axis...  19.8 us
    all_to_all x2, starting transfers between devices, from_everyone(): lax.all_to_all(jnp.broadcast_to(value[None], (peers, *value.shape)), axis...  14.1 us
    dot_general x1, matrix products, local(): lax.dot_general(out_grad, hidden, (((0,), (0,)), ((), ())), preferred_ele...  6.27 us
    dot_general x1, matrix products, local(): lax.dot_general(out_grad, weight_whole, (((1,), (1,)), ((), ())), preferr...  6.14 us
  transfers between devices with their start and end apart: 4, of which 4 were waited for; matrix products, arithmetic and copies ran while one was open for 3% of the time, Pallas kernels for 0%

commit v1 on v0

v1 whole, which is shorter than its diff:
```python
import functools

import jax
import jax.numpy as jnp
from jax import lax
from jax.experimental import pallas as pl
from jax.experimental.pallas import tpu as pltpu
from jax.sharding import Mesh
from jax.sharding import PartitionSpec as P


D = 2048
FS = ("fs_0", "fs_1")
REP_FS = ("rep", "fs_0", "fs_1")
HOPS = (1, -1, 2)


def swap(blocks, axis):
    return lax.all_to_all(blocks, axis, 0, 0, tiled=True)


def moved(value, hops):
    reps, depth, tp = (lax.axis_size(a) for a in ("rep", "fs_0", "tp"))
    ring = reps * depth
    pairs = []
    for z in range(ring):
        for t in range(tp):
            by = -hops if abs(hops) == 2 and t % 2 else hops
            pairs.append((z * tp + t, (z + by) % ring * tp + t))
    return lax.ppermute(value, ("rep", "fs_0", "tp"), pairs)


def in_vmem(kernel, shapes, *values):
    spec = pl.BlockSpec(memory_space=pltpu.VMEM)
    return pl.pallas_call(
        kernel,
        in_specs=[spec] * len(values),
        out_specs=[spec] * len(shapes),
        out_shape=[pltpu.VMEM(shape, kind) for shape, kind in shapes],
    )(*(pltpu.with_memory_space_constraint(v, pltpu.VMEM) for v in values))


def partial_kernel(first_ref, gate_ref, up_ref, cot_ref, out1, out2, out3, own, hidden_ref):
    step = pl.program_id(0)

    @pl.when(step == 0)
    def _():
        gate = gate_ref[...].astype(jnp.float32)
        hidden = gate * jax.nn.sigmoid(gate) * up_ref[...].astype(jnp.float32)
        hidden_ref[...] = hidden.T.astype(jnp.bfloat16)

    for k, out in enumerate((out1, out2, out3, own)):

        @pl.when(step == k)
        def _(out=out):
            part = jnp.dot(hidden_ref[...], cot_ref[...], preferred_element_type=jnp.float32)
            out[...] = part.astype(out.dtype)


def partial_grad(first, gate, up, cot):
    tokens, units = gate.shape
    cols = cot.shape[1] // 4

    def block(i, first):
        hops = jnp.where(i == 0, HOPS[0], jnp.where(i == 1, HOPS[1], jnp.where(i == 2, HOPS[2], 0)))
        return (0, lax.rem(first[0] + hops + 4, 4))

    whole = lambda i, first: (0, 0)
    return pl.pallas_call(
        partial_kernel,
        grid_spec=pltpu.PrefetchScalarGridSpec(
            num_scalar_prefetch=1,
            grid=(4,),
            in_specs=[
                pl.BlockSpec((tokens, units), whole),
                pl.BlockSpec((tokens, units), whole),
                pl.BlockSpec((tokens, cols), block),
            ],
            out_specs=[pl.BlockSpec(memory_space=pltpu.VMEM)] * 4,
            scratch_shapes=[pltpu.VMEM((units, tokens), jnp.bfloat16)],
        ),
        out_shape=[pltpu.VMEM((units, cols), jnp.bfloat16)] * 3
        + [pltpu.VMEM((units, cols), jnp.float32)],
        compiler_params=pltpu.CompilerParams(dimension_semantics=("arbitrary",)),
        name="partial_grad",
    )(first, gate, up, cot)


def window_kernel(own_ref, got1, got2, got3, out_ref):
    total = own_ref[...]
    for got in (got1, got2, got3):
        total = total + got[...].astype(jnp.float32)
    out_ref[...] = total.T.reshape(out_ref.shape).astype(out_ref.dtype)


def sum_kernel(got_ref, out_ref):
    total = jnp.sum(got_ref[...].astype(jnp.float32), axis=0)
    out_ref[...] = jnp.broadcast_to(total.astype(out_ref.dtype)[None], out_ref.shape)


def finish_kernel(factor, got_ref, grad_ref, rows_ref):
    grad = jnp.sum(got_ref[...].astype(jnp.float32), axis=0) * factor
    grad_ref[...] = grad
    rows_ref[...] = jnp.broadcast_to(
        jnp.sum(grad * grad, axis=0, keepdims=True)[None], rows_ref.shape
    )


def input_kernel(first_ref, gate_ref, up_ref, cot_ref, w0, w1, w2, w3, dgate_ref, dup_ref):
    first = first_ref[0]
    rows = w0.shape[0]
    dhid = None
    for hops, w in zip((0, 1, -1, 2), (w0, w1, w2, w3)):
        at = pl.multiple_of(lax.rem(first - hops + 4, 4) * rows, rows)
        term = jnp.dot(cot_ref[:, pl.ds(at, rows)], w[...], preferred_element_type=jnp.float32)
        dhid = term if dhid is None else dhid + term
    gate = gate_ref[...].astype(jnp.float32)
    up = up_ref[...].astype(jnp.float32)
    sig = jax.nn.sigmoid(gate)
    dup_ref[...] = (dhid * (gate * sig)).astype(jnp.bfloat16)
    dgate_ref[...] = (dhid * up * sig * (1.0 + gate * (1.0 - sig))).astype(jnp.bfloat16)


def input_grads(first, gate, up, cot, weights, step=256):
    tokens, units = gate.shape
    width = cot.shape[1]
    rows = lambda i, first: (i, 0)
    return pl.pallas_call(
        input_kernel,
        grid_spec=pltpu.PrefetchScalarGridSpec(
            num_scalar_prefetch=1,
            grid=(tokens // step,),
            in_specs=[
                pl.BlockSpec((step, units), rows),
                pl.BlockSpec((step, units), rows),
                pl.BlockSpec((step, width), rows),
            ]
            + [pl.BlockSpec(memory_space=pltpu.VMEM)] * 4,
            out_specs=[pl.BlockSpec((step, units), rows)] * 2,
        ),
        out_shape=[jax.ShapeDtypeStruct((tokens, units), jnp.bfloat16)] * 2,
        compiler_params=pltpu.CompilerParams(dimension_semantics=("arbitrary",)),
        name="input_grads",
    )(first, gate, up, cot, *(pltpu.with_memory_space_constraint(w, pltpu.VMEM) for w in weights))


def local(gate_pre, up_pre, out_grad, w_down):
    peers, reps, high = (lax.axis_size(a) for a in (FS, "rep", "fs_1"))
    factor = float(out_grad.shape[0] * reps * peers) ** (-0.5)
    units, cols = w_down.shape
    kind = jnp.bfloat16
    first = lax.axis_index("fs_0").astype(jnp.int32)[None]

    copies = jnp.broadcast_to(w_down.T[None], (high, cols, units))
    mine = swap(copies, "fs_1").reshape(-1, units)
    *away, own = partial_grad(first, gate_pre, up_pre, out_grad)
    got = [moved(part, hops) for part, hops in zip(away, HOPS)]
    (part,) = in_vmem(window_kernel, [((high, cols, units), kind)], own, *got)
    got = swap(part, "fs_1")
    weights = [mine] + [moved(mine, hops) for hops in HOPS]
    (total,) = in_vmem(sum_kernel, [((reps, cols, units), kind)], got)
    got = swap(total, "rep")
    grad, rows = in_vmem(
        functools.partial(finish_kernel, factor),
        [((cols, units), jnp.float32), ((peers, 1, units), jnp.float32)],
        got,
    )
    energy = jnp.sum(swap(rows, FS), axis=(0, 1)) / D
    d_gate, d_up = input_grads(first, gate_pre, up_pre, out_grad, weights)
    return d_gate, d_up, grad.T, energy


def solution(mesh):
    torus = Mesh(
        mesh.devices.reshape(mesh.shape["rep"], 4, 8, mesh.shape["tp"]),
        ("rep", "fs_0", "fs_1", "tp"),
    )
    placed = (P(REP_FS, "tp"), P(REP_FS, "tp"), P(REP_FS, None), P("tp", FS))
    return jax.shard_map(
        local,
        mesh=torus,
        in_specs=placed,
        out_specs=(P(REP_FS, "tp"), P(REP_FS, "tp"), P("tp", FS), P("tp")),
        check_vma=False,
    )
```

time: 206 us -> 118 us (0.57)
  the two profiles are of different devices: /device:TPU:4 before, /device:TPU:131 now
where the time goes in v1:
time: 118 us; the launch traced here: 117 us
  starting transfers between devices  45.5 us (39%)
  waiting for transfers between devices  38.3 us (32%)
  blocking collectives  17.8 us (15%)
  Pallas kernels  12.8 us (11%)
  local copies, waits for them, and re-layouts  1.43 us (1%)
    ppermute x6, starting transfers between devices, moved(): return lax.ppermute(value, ('rep', 'fs_0', 'tp'), pairs)  31.3 us
    ppermute x6, waiting for transfers between devices, moved(): return lax.ppermute(value, ('rep', 'fs_0', 'tp'), pairs)  26.8 us
    all_to_all x1, blocking collectives, swap(): return lax.all_to_all(blocks, axis, 0, 0, tiled=True)  17.8 us
    all_to_all x3, starting transfers between devices, swap(): return lax.all_to_all(blocks, axis, 0, 0, tiled=True)  14.3 us
    all_to_all x3, waiting for transfers between devices, swap(): return lax.all_to_all(blocks, axis, 0, 0, tiled=True)  11.5 us
    pallas_call x1, Pallas kernels, input_grads(): pl.pallas_call(input_kernel, grid_spec=pltpu.PrefetchScalarGridSpec(num_s...  6.19 us
    pallas_call x1, Pallas kernels, partial_grad(): pl.pallas_call(partial_kernel, grid_spec=pltpu.PrefetchScalarGridSpec(num...  4.97 us
  transfers between devices with their start and end apart: 9, of which 5 were waited for; matrix products, arithmetic and copies ran while one was open for 1% of the time, Pallas kernels for 6%

profile of v1, /device:TPU:131, one launch (start us, length us, event | category | flops | bytes accessed | tf_op | source)
XLA Modules:
  0.0 117.3 jit_solution(8988486806064700870)
XLA Ops:
  0.6 0.0 copy-start
  0.6 5.0 %partial_grad.1 = (bf16[384,512]{1,0:T(8,128)(2,1)S(1)}, bf16[384,512]{1,0:T(8,128)(2,1)S(1)}, bf16[384,512]{1,0:T(8,128)(2,1)S(1)}, f32[384,512]{1,0:T(8,128)S(1)}) custom-call(s32[1]{0:T(128)} %bitcast.first_ref, bf16[1024,384]{1,0:T(8,128)(2,1)} %gate_ref.3, bf16[1024,384]{1,0:T(8,128)(2,1)} %up_ref.3, bf16[1024,2048]{1,0:T(8,128)(2,1)} %cot_ref.3), custom_call_target="tpu_custom_call" | custom-call | tf_op jit(solution)/shard_map/partial_grad/pallas_call | solution.py:69
  5.6 4.0 %collective-permute-start.3 = (bf16[384,512]{1,0:T(8,128)(2,1)S(1)}, bf16[384,512]{1,0:T(8,128)(2,1)S(1)}, u32[]{:S(2)}, u32[]{:S(2)}) collective-permute-start(bf16[384,512]{1,0:T(8,128)(2,1)S(1)} %get-tuple-element.15), channel_id=1, source_target_pairs={{0,64},{1,65},{2,66},{3,67},{4,68},{5,69},{6,70},{7,71},{64,128},{... | collective-permute-start | bytes 1179656 | tf_op jit(solution)/shard_map/ppermute | solution.py:30
  9.6 1.9 %collective-permute-start.4 = (bf16[384,512]{1,0:T(8,128)(2,1)S(1)}, bf16[384,512]{1,0:T(8,128)(2,1)S(1)}, u32[]{:S(2)}, u32[]{:S(2)}) collective-permute-start(bf16[384,512]{1,0:T(8,128)(2,1)S(1)} %get-tuple-element.16), channel_id=1, source_target_pairs={{0,704},{1,705},{2,706},{3,707},{4,708},{5,709},{6,710},{7,711},{6... | collective-permute-start | bytes 1179656 | tf_op jit(solution)/shard_map/ppermute | solution.py:30
  11.6 10.7 %collective-permute-start.5 = (bf16[384,512]{1,0:T(8,128)(2,1)S(1)}, bf16[384,512]{1,0:T(8,128)(2,1)S(1)}, u32[]{:S(2)}, u32[]{:S(2)}) collective-permute-start(bf16[384,512]{1,0:T(8,128)(2,1)S(1)} %get-tuple-element.17), channel_id=1, source_target_pairs={{0,128},{1,641},{2,130},{3,643},{4,132},{5,645},{6,134},{7,647},{6... | collective-permute-start | bytes 1179656 | tf_op jit(solution)/shard_map/ppermute | solution.py:30
  22.2 0.0 collective-permute-done.3.got1
  22.3 1.1 collective-permute-done.4.got2
  23.4 11.7 %collective-permute-done.5.got3 = bf16[384,512]{1,0:T(8,128)(2,1)S(1)} collective-permute-done((bf16[384,512]{1,0:T(8,128)(2,1)S(1)}, bf16[384,512]{1,0:T(8,128)(2,1)S(1)}, u32[]{:S(2)}, u32[]{:S(2)}) %collective-permute-start.5) | collective-permute-done | bytes 393248 | tf_op jit(solution)/shard_map/ppermute | solution.py:30
  35.0 0.2 shard_map.75
  35.3 17.8 %all_to_all.20.got_ref = bf16[8,64,384]{2,1,0:T(8,128)(2,1)S(1)} all-to-all(bf16[8,64,384]{2,1,0:T(8,128)(2,1)S(1)} %shard_map.75), channel_id=1, replica_groups=mesh['rep'=3,'fs_0'=4,'fs_1'=8,'tp'=8] {'fs_1'}, dimensions={0} | all-to-all | bytes 786432 | tf_op jit(solution)/shard_map/all_to_all | solution.py:19
  53.1 0.0 copy-done
  53.1 0.8 broadcast_in_dim.10
  53.9 3.5 %all-to-all-start = ((bf16[8,64,384]{2,1,0:T(8,128)(2,1)}), bf16[8,64,384]{2,1,0:T(8,128)(2,1)S(1)}, u32[]{:S(2)}, u32[]{:S(2)}) async-start(bf16[8,64,384]{2,1,0:T(8,128)(2,1)} %broadcast_in_dim.10), calls=%async_computation | async-start | bytes 786432 | tf_op jit(solution)/shard_map/all_to_all | solution.py:19
  57.3 0.7 shard_map.76
  58.1 11.5 %all-to-all-done = bf16[8,64,384]{2,1,0:T(8,128)(2,1)S(1)} async-done(((bf16[8,64,384]{2,1,0:T(8,128)(2,1)}), bf16[8,64,384]{2,1,0:T(8,128)(2,1)S(1)}, u32[]{:S(2)}, u32[]{:S(2)}) %all-to-all-start) | async-done | bytes 393248 | tf_op jit(solution)/shard_map/all_to_all | solution.py:19
  69.6 6.4 %all-to-all-start.2 = ((bf16[3,64,384]{2,1,0:T(8,128)(2,1)}), bf16[3,64,384]{2,1,0:T(8,128)(2,1)S(1)}, u32[]{:S(2)}, u32[]{:S(2)}) async-start(bf16[3,64,384]{2,1,0:T(8,128)(2,1)} %shard_map.76), calls=%async_computation.2 | async-start | bytes 294912 | tf_op jit(solution)/shard_map/all_to_all | solution.py:19
  76.0 2.2 %collective-permute-start = (bf16[512,384]{1,0:T(8,128)(2,1)S(1)}, bf16[512,384]{1,0:T(8,128)(2,1)S(1)}, u32[]{:S(2)}, u32[]{:S(2)}) collective-permute-start(bf16[512,384]{1,0:T(8,128)(2,1)S(1)} %bitcast.5), channel_id=1, source_target_pairs={{0,64},{1,65},{2,66},{3,67},{4,68},{5,69},{6,70},{7,71},{64,128},{... | collective-permute-start | bytes 1179656 | tf_op jit(solution)/shard_map/ppermute | solution.py:30
  78.2 5.7 %collective-permute-start.1 = (bf16[512,384]{1,0:T(8,128)(2,1)S(1)}, bf16[512,384]{1,0:T(8,128)(2,1)S(1)}, u32[]{:S(2)}, u32[]{:S(2)}) collective-permute-start(bf16[512,384]{1,0:T(8,128)(2,1)S(1)} %bitcast.6), channel_id=1, source_target_pairs={{0,704},{1,705},{2,706},{3,707},{4,708},{5,709},{6,710},{7,711},{6... | collective-permute-start | bytes 1179656 | tf_op jit(solution)/shard_map/ppermute | solution.py:30
  83.9 6.8 %collective-permute-start.2 = (bf16[512,384]{1,0:T(8,128)(2,1)S(1)}, bf16[512,384]{1,0:T(8,128)(2,1)S(1)}, u32[]{:S(2)}, u32[]{:S(2)}) collective-permute-start(bf16[512,384]{1,0:T(8,128)(2,1)S(1)} %bitcast.7), channel_id=1, source_target_pairs={{0,128},{1,641},{2,130},{3,643},{4,132},{5,645},{6,134},{7,647},{6... | collective-permute-start | bytes 1179656 | tf_op jit(solution)/shard_map/ppermute | solution.py:30
  90.7 0.0 all-to-all-done.2.got_ref
  90.7 0.7 shard_map.77
  91.4 4.4 %all-to-all-start.3 = ((f32[32,1,384]{2,1,0:T(1,128)}), f32[32,1,384]{2,1,0:T(1,128)S(1)}, u32[]{:S(2)}, u32[]{:S(2)}) async-start(f32[32,1,384]{2,1,0:T(1,128)} %get-tuple-element.19), calls=%async_computation.3 | async-start | bytes 98304 | tf_op jit(solution)/shard_map/all_to_all | solution.py:19
  95.8 0.0 collective-permute-done.w1
  95.8 2.1 %collective-permute-done.1.w2 = bf16[512,384]{1,0:T(8,128)(2,1)S(1)} collective-permute-done((bf16[512,384]{1,0:T(8,128)(2,1)S(1)}, bf16[512,384]{1,0:T(8,128)(2,1)S(1)}, u32[]{:S(2)}, u32[]{:S(2)}) %collective-permute-start.1) | collective-permute-done | bytes 393248 | tf_op jit(solution)/shard_map/ppermute | solution.py:30
  97.9 11.9 %collective-permute-done.2.w3 = bf16[512,384]{1,0:T(8,128)(2,1)S(1)} collective-permute-done((bf16[512,384]{1,0:T(8,128)(2,1)S(1)}, bf16[512,384]{1,0:T(8,128)(2,1)S(1)}, u32[]{:S(2)}, u32[]{:S(2)}) %collective-permute-start.2) | collective-permute-done | bytes 393248 | tf_op jit(solution)/shard_map/ppermute | solution.py:30
  109.8 6.2 %input_grads.1 = (bf16[1024,384]{1,0:T(8,128)(2,1)}, bf16[1024,384]{1,0:T(8,128)(2,1)}) custom-call(s32[1]{0:T(128)} %bitcast.first_ref, bf16[1024,384]{1,0:T(8,128)(2,1)} %gate_ref.3, bf16[1024,384]{1,0:T(8,128)(2,1)} %up_ref.3, bf16[1024,2048]{1,0:T(8,128)(2,1)} %cot_ref.3, bf16[512,384]{1,0:T(8,128)(2,1)S(1)} %bitcast.8, ...), custom_call_target="tpu_custom_call" | custom-call | tf_op jit(solution)/shard_map/input_grads/pallas_call | solution.py:128
  116.0 0.6 copy.8
  116.7 0.0 all-to-all-done.3
  116.7 0.1 reduce_sum.9
  116.7 0.6 broadcast_multiply_fusion
Async XLA Ops:
  0.6 52.5 %copy-start = (bf16[384,64]{0,1:T(8,128)(2,1)S(1)}, bf16[384,64]{0,1:T(8,128)(2,1)}, u32[]{:S(2)}) copy-start(bf16[384,64]{0,1:T(8,128)(2,1)} %param.7) | copy-start | bytes 147460
  5.6 16.6 %collective-permute-start.3 = (bf16[384,512]{1,0:T(8,128)(2,1)S(1)}, bf16[384,512]{1,0:T(8,128)(2,1)S(1)}, u32[]{:S(2)}, u32[]{:S(2)}) collective-permute-start(bf16[384,512]{1,0:T(8,128)(2,1)S(1)} %get-tuple-element.15), channel_id=1, source_target_pairs={{0,64},{1,65},{2,66},{3,67},{4,68},{5,69},{6,70},{7,71},{64,128},{... | collective-permute-start | bytes 1179656 | tf_op jit(solution)/shard_map/ppermute | solution.py:30
  9.6 13.7 %collective-permute-start.4 = (bf16[384,512]{1,0:T(8,128)(2,1)S(1)}, bf16[384,512]{1,0:T(8,128)(2,1)S(1)}, u32[]{:S(2)}, u32[]{:S(2)}) collective-permute-start(bf16[384,512]{1,0:T(8,128)(2,1)S(1)} %get-tuple-element.16), channel_id=1, source_target_pairs={{0,704},{1,705},{2,706},{3,707},{4,708},{5,709},{6,710},{7,711},{6... | collective-permute-start | bytes 1179656 | tf_op jit(solution)/shard_map/ppermute | solution.py:30
  11.6 23.5 %collective-permute-start.5 = (bf16[384,512]{1,0:T(8,128)(2,1)S(1)}, bf16[384,512]{1,0:T(8,128)(2,1)S(1)}, u32[]{:S(2)}, u32[]{:S(2)}) collective-permute-start(bf16[384,512]{1,0:T(8,128)(2,1)S(1)} %get-tuple-element.17), channel_id=1, source_target_pairs={{0,128},{1,641},{2,130},{3,643},{4,132},{5,645},{6,134},{7,647},{6... | collective-permute-start | bytes 1179656 | tf_op jit(solution)/shard_map/ppermute | solution.py:30
  53.9 15.7 %all-to-all-start = ((bf16[8,64,384]{2,1,0:T(8,128)(2,1)}), bf16[8,64,384]{2,1,0:T(8,128)(2,1)S(1)}, u32[]{:S(2)}, u32[]{:S(2)}) async-start(bf16[8,64,384]{2,1,0:T(8,128)(2,1)} %broadcast_in_dim.10), calls=%async_computation | async-start | bytes 786432 | tf_op jit(solution)/shard_map/all_to_all | solution.py:19
  69.6 21.1 %all-to-all-start.2 = ((bf16[3,64,384]{2,1,0:T(8,128)(2,1)}), bf16[3,64,384]{2,1,0:T(8,128)(2,1)S(1)}, u32[]{:S(2)}, u32[]{:S(2)}) async-start(bf16[3,64,384]{2,1,0:T(8,128)(2,1)} %shard_map.76), calls=%async_computation.2 | async-start | bytes 294912 | tf_op jit(solution)/shard_map/all_to_all | solution.py:19
  76.0 19.8 %collective-permute-start = (bf16[512,384]{1,0:T(8,128)(2,1)S(1)}, bf16[512,384]{1,0:T(8,128)(2,1)S(1)}, u32[]{:S(2)}, u32[]{:S(2)}) collective-permute-start(bf16[512,384]{1,0:T(8,128)(2,1)S(1)} %bitcast.5), channel_id=1, source_target_pairs={{0,64},{1,65},{2,66},{3,67},{4,68},{5,69},{6,70},{7,71},{64,128},{... | collective-permute-start | bytes 1179656 | tf_op jit(solution)/shard_map/ppermute | solution.py:30
  78.2 19.7 %collective-permute-start.1 = (bf16[512,384]{1,0:T(8,128)(2,1)S(1)}, bf16[512,384]{1,0:T(8,128)(2,1)S(1)}, u32[]{:S(2)}, u32[]{:S(2)}) collective-permute-start(bf16[512,384]{1,0:T(8,128)(2,1)S(1)} %bitcast.6), channel_id=1, source_target_pairs={{0,704},{1,705},{2,706},{3,707},{4,708},{5,709},{6,710},{7,711},{6... | collective-permute-start | bytes 1179656 | tf_op jit(solution)/shard_map/ppermute | solution.py:30
  83.9 26.0 %collective-permute-start.2 = (bf16[512,384]{1,0:T(8,128)(2,1)S(1)}, bf16[512,384]{1,0:T(8,128)(2,1)S(1)}, u32[]{:S(2)}, u32[]{:S(2)}) collective-permute-start(bf16[512,384]{1,0:T(8,128)(2,1)S(1)} %bitcast.7), channel_id=1, source_target_pairs={{0,128},{1,641},{2,130},{3,643},{4,132},{5,645},{6,134},{7,647},{6... | collective-permute-start | bytes 1179656 | tf_op jit(solution)/shard_map/ppermute | solution.py:30
  91.4 25.3 %all-to-all-start.3 = ((f32[32,1,384]{2,1,0:T(1,128)}), f32[32,1,384]{2,1,0:T(1,128)S(1)}, u32[]{:S(2)}, u32[]{:S(2)}) async-start(f32[32,1,384]{2,1,0:T(1,128)} %get-tuple-element.19), calls=%async_computation.3 | async-start | bytes 98304 | tf_op jit(solution)/shard_map/all_to_all | solution.py:19
